TPU v7x, 32 devices: a whole 2x2x4 slice. The times are simulated.
32 devices in a mesh: sp: 8 (over z, x), tp: 4 (over y, core).
Axes of the slice: x: 2, y: 2, z: 4, core: 2. Of those that a mesh axis runs over, the one named last changes fastest.
Arguments:
- mixer_out: bfloat16 [1024, 2048], P('sp', 'tp'), may hold values from -12 to 12
- layer_grad: bfloat16 [1024, 2048], P('sp', 'tp'), may hold values from -6 to 6
- row_scale: float32 [1024], P('sp'), may hold values from 0.3 to 3
- norm_gain: bfloat16 [2048], replicated, may hold values from 0.099609375 to 1.8984375
- routes: int32 [1024, 2], P('sp'), may hold values from 0 to 7, all different within a row; in each aligned block of 128 rows (0 to 127, 128 to 255, ...) at most 64 rows name the same one
- route_weight: float32 [1024, 2], P('sp'), may hold values from 0.05 to 0.35
- expert_gate: bfloat16 [8, 3584, 2048], P('sp', 'tp'), may hold values from -0.125 to 0.125
- expert_up: bfloat16 [8, 3584, 2048], P('sp', 'tp'), may hold values from -0.125 to 0.125
- expert_down: bfloat16 [8, 3584, 2048], P('sp', 'tp'), may hold values from -0.09375 to 0.09375
- query_rows: bfloat16 [1024, 1024], P('sp', 'tp'), may hold values from -6 to 6
- key_rows: bfloat16 [1024, 1024], P('sp', 'tp'), may hold values from -6 to 6
- value_rows: bfloat16 [1024, 1024], P('sp', 'tp'), may hold values from -6 to 6
- retained: bfloat16 [1024, 1024], P('sp', 'tp'), may hold values from -6 to 6
- log_decay: float32 [16, 1024], P('tp', 'sp'), may hold values from -0.8 to 0
- entry_state: float32 [8, 16, 64, 64], P('sp', 'tp'), may hold values from -12 to 12
- out_proj: bfloat16 [1024, 2048], P('tp'), may hold values from -0.1875 to 0.1875
Outputs:
- grad_up: bfloat16 [8, 3584, 2048], P('sp', 'tp')
- grad_down: bfloat16 [8, 3584, 2048], P('sp', 'tp')
- grad_proj: float32 [2048, 1024], P('sp', 'tp')
- grad_query: bfloat16 [1024, 1024], P('sp', 'tp')
- grad_key: bfloat16 [1024, 1024], P('sp', 'tp')
- grad_value: bfloat16 [1024, 1024], P('sp', 'tp')
- stream_grad: bfloat16 [1024, 2048], P('sp', 'tp')
Inputs may be any that keep to these rules, and one draw needn't show every extreme that they name: `routes`: each row names 2 different experts. Among the entries of one block of 128 consecutive rows no expert appears more than 64 times, and in every draw some block names some expert exactly 64 times.
All inputs are finite; a program needn't handle non-finite values.
Results may differ from a plain program's by a relative error of at most 0.025.
Values may be sent and summed in bfloat16 or wider, within the bound.
A program may use at most 64 MiB of HBM per device.

v0:
```python
import jax
import jax.numpy as jnp
from jax import lax
from jax.sharding import PartitionSpec as P


def prefix(array, axis, combine, identity):
    devices, position = (lax.axis_size(axis), lax.axis_index(axis))
    everything = jax.tree.map(lambda part: lax.all_gather(part, axis), array)
    start = jax.tree.map(
        lambda part, zero: jnp.broadcast_to(jnp.asarray(zero, part.dtype), part.shape),
        array,
        identity,
    )

    def step(k, before):
        at = devices - 1 - k
        reached = at > position
        new = combine(before, jax.tree.map(lambda part: part[at], everything))
        return jax.tree.map(lambda a, b: jnp.where(reached, a, b), new, before)

    return lax.fori_loop(0, devices, step, start)


def contract_last(first_op, second_op):
    return lax.dot_general(
        first_op, second_op, (((1,), (1,)), ((), ())), preferred_element_type=jnp.float32
    )


def contract_first(first_op, second_op):
    return lax.dot_general(
        first_op, second_op, (((0,), (0,)), ((), ())), preferred_element_type=jnp.float32
    )


def slot_sources(routes, experts, capacity):
    flat_ids = routes.reshape(-1)
    entries = flat_ids.shape[0]
    onehot = (flat_ids[:, None] == jnp.arange(experts, dtype=jnp.int32)[None, :]).astype(jnp.int32)
    rank_in = jnp.sum(onehot * (jnp.cumsum(onehot, axis=0) - 1), axis=1)
    slot_ids = flat_ids * capacity + rank_in
    matches = slot_ids[None, :] == jnp.arange(experts * capacity, dtype=jnp.int32)[:, None]
    sources = jnp.sum(jnp.where(matches, jnp.arange(entries, dtype=jnp.int32)[None, :], 0), axis=1)
    sources = jnp.where(jnp.any(matches, axis=1), sources, entries)
    return (slot_ids, sources)


def pick_rows(row_block, sources):
    padded = jnp.concatenate(
        [row_block, jnp.zeros((1, row_block.shape[1]), row_block.dtype)], axis=0
    )
    return jnp.take(padded, sources, axis=0)


def span_terms(head_queries, head_keys, head_values, head_gradient, decay_head, incoming_state):
    scale = head_queries.shape[-1] ** (-0.5)
    length = decay_head.shape[1]
    cumul = jnp.cumsum(decay_head, axis=1)
    places = jnp.arange(length)
    causal = (places[:, None] >= places[None, :])[None, :, :]
    spread = cumul[:, :, None] - cumul[:, None, :]
    weights = jnp.where(causal, jnp.exp(jnp.where(causal, spread, 0.0)), 0.0)
    scores = (
        scale
        * jnp.einsum("thd,shd->hts", head_queries, head_keys, precision=lax.Precision.HIGHEST)
        * weights
    )
    pressure = (
        scale
        * jnp.einsum("thd,shd->hts", head_gradient, head_values, precision=lax.Precision.HIGHEST)
        * weights
    )
    grad_query = jnp.einsum("hts,shd->thd", pressure, head_keys, precision=lax.Precision.HIGHEST)
    grad_key = jnp.einsum("hts,thd->shd", pressure, head_queries, precision=lax.Precision.HIGHEST)
    grad_value = jnp.einsum("hts,thd->shd", scores, head_gradient, precision=lax.Precision.HIGHEST)
    ascending_decay = jnp.exp(cumul).T
    grad_query = grad_query + scale * ascending_decay[:, :, None] * jnp.einsum(
        "joy,oiy->joi", head_gradient, incoming_state, precision=lax.Precision.HIGHEST
    )
    state_update = jnp.einsum(
        "olb,oli->lbi",
        head_queries * ascending_decay[:, :, None],
        head_gradient,
        precision=lax.Precision.HIGHEST,
    )
    survive = jnp.exp(cumul[:, -1])
    falling = jnp.exp(cumul[:, -1:] - cumul).T
    return (grad_query, grad_key, grad_value, state_update, survive, falling)


def add_carried(grad_key, grad_value, head_keys, head_values, falling, carried_over_state):
    scale = head_keys.shape[-1] ** (-0.5)
    grad_key = grad_key + scale * falling[:, :, None] * jnp.einsum(
        "upy,ruy->rup", carried_over_state, head_values, precision=lax.Precision.HIGHEST
    )
    grad_value = grad_value + scale * falling[:, :, None] * jnp.einsum(
        "rzw,erz->erw", carried_over_state, head_keys, precision=lax.Precision.HIGHEST
    )
    return (grad_key, grad_value)


def combine_spans(earlier, later_run):
    return (later_run[0] * earlier[0], later_run[1] + later_run[0][:, None, None] * earlier[1])


def body(
    mixer_out,
    layer_grad,
    row_scale,
    norm_gain,
    routes,
    route_weight,
    expert_gate,
    expert_up,
    expert_down,
    query_rows,
    key_rows,
    value_rows,
    retained,
    log_decay,
    entry_state,
    out_proj,
):
    experts = lax.axis_size("sp")
    tp_count = lax.axis_size("tp")
    tokens_here, columns = mixer_out.shape
    fanout = routes.shape[1]
    capacity = 2 * fanout * tokens_here // experts
    slot_ids, sources = slot_sources(routes, experts, capacity)
    gain_all = norm_gain.astype(jnp.float32)
    gain_cols = lax.dynamic_slice_in_dim(gain_all, lax.axis_index("tp") * columns, columns)
    scaled = mixer_out.astype(jnp.float32) * row_scale[:, None]
    normed = (scaled * gain_cols[None, :]).astype(jnp.bfloat16)
    weight_col = route_weight.reshape(-1)[:, None]
    weighted = (weight_col * jnp.repeat(layer_grad.astype(jnp.float32), fanout, axis=0)).astype(
        jnp.bfloat16
    )
    send_normed = pick_rows(jnp.repeat(normed, fanout, axis=0), sources).reshape(
        experts, capacity, columns
    )
    send_grad = pick_rows(weighted, sources).reshape(experts, capacity, columns)
    got_normed, got_grad = (
        lax.all_to_all(send_normed, "sp", split_axis=0, concat_axis=0, tiled=True),
        lax.all_to_all(send_grad, "sp", split_axis=0, concat_axis=0, tiled=True),
    )
    gate_weight = expert_gate[0]
    up_weight = expert_up[0]
    down_weight = expert_down[0]
    model_width = gate_weight.shape[1]
    full_normed, full_grad = (
        lax.all_gather(got_normed, "tp", axis=2, tiled=True),
        lax.all_gather(got_grad, "tp", axis=2, tiled=True),
    )
    normed_rows = full_normed.reshape(-1, model_width)
    grad_rows = full_grad.reshape(-1, model_width)
    gate_pre = contract_last(normed_rows, gate_weight)
    up_pre = contract_last(normed_rows, up_weight)
    act_grad = contract_last(grad_rows, down_weight)
    sigmoid_gate = jax.nn.sigmoid(gate_pre)
    silu_gate = gate_pre * sigmoid_gate
    activation = (silu_gate * up_pre).astype(jnp.bfloat16)
    grad_down = contract_first(activation, grad_rows).astype(jnp.bfloat16)[None]
    up_grad = (act_grad * silu_gate).astype(jnp.bfloat16)
    gate_grad = (act_grad * up_pre * sigmoid_gate * (1.0 + gate_pre * (1.0 - sigmoid_gate))).astype(
        jnp.bfloat16
    )
    grad_up = contract_first(up_grad, normed_rows).astype(jnp.bfloat16)[None]
    partial_value = jnp.dot(gate_grad, gate_weight, preferred_element_type=jnp.float32) + jnp.dot(
        up_grad, up_weight, preferred_element_type=jnp.float32
    )
    shares = lax.psum_scatter(
        partial_value.astype(jnp.bfloat16), "tp", scatter_dimension=1, tiled=True
    )
    returned = lax.all_to_all(
        shares.reshape(experts, capacity, columns), "sp", split_axis=0, concat_axis=0, tiled=True
    )
    per_route = jnp.take(returned.reshape(experts * capacity, columns), slot_ids, axis=0)
    hidden_grad = jnp.sum(
        per_route.reshape(tokens_here, fanout, columns).astype(jnp.float32), axis=1
    ).astype(jnp.bfloat16)
    attend = gain_cols[None, :] * hidden_grad.astype(jnp.float32)
    total_dot = lax.psum(jnp.sum(scaled * attend, axis=1), "tp")
    mean_dot = total_dot[:, None] / (columns * tp_count)
    stream_grad = (
        layer_grad.astype(jnp.float32) + row_scale[:, None] * (attend - scaled * mean_dot)
    ).astype(jnp.bfloat16)
    stream_full = lax.all_gather(stream_grad, "tp", axis=1, tiled=True)
    out_grad = contract_last(stream_full, out_proj).astype(jnp.bfloat16)
    head_count = entry_state.shape[1]
    head_dim = entry_state.shape[-1]

    def split_heads(block):
        return block.astype(jnp.float32).reshape(tokens_here, head_count, head_dim)

    head_keys = split_heads(key_rows)
    head_values = split_heads(value_rows)
    grad_query, grad_key, grad_value, state_update, survive, falling = span_terms(
        split_heads(query_rows),
        head_keys,
        head_values,
        split_heads(out_grad),
        log_decay,
        entry_state[0],
    )
    carried_over_state = prefix(
        (survive, state_update),
        "sp",
        combine_spans,
        (jnp.ones_like(survive), jnp.zeros_like(state_update)),
    )[1]
    grad_key, grad_value = add_carried(
        grad_key, grad_value, head_keys, head_values, falling, carried_over_state
    )
    grad_proj = lax.psum_scatter(
        contract_first(stream_full, retained).astype(jnp.bfloat16),
        "sp",
        scatter_dimension=0,
        tiled=True,
    ).astype(jnp.float32)
    ret_cols = head_count * head_dim
    return (
        grad_up,
        grad_down,
        grad_proj,
        grad_query.reshape(tokens_here, ret_cols).astype(jnp.bfloat16),
        grad_key.reshape(tokens_here, ret_cols).astype(jnp.bfloat16),
        grad_value.reshape(tokens_here, ret_cols).astype(jnp.bfloat16),
        stream_grad,
    )


def solution(mesh):
    in_specs = (
        P("sp", "tp"),
        P("sp", "tp"),
        P("sp"),
        P(),
        P("sp", None),
        P("sp", None),
        P("sp", "tp", None),
        P("sp", "tp", None),
        P("sp", "tp", None),
        P("sp", "tp"),
        P("sp", "tp"),
        P("sp", "tp"),
        P("sp", "tp"),
        P("tp", "sp"),
        P("sp", "tp", None, None),
        P("tp", None),
    )
    out_specs = (
        P("sp", "tp", None),
        P("sp", "tp", None),
        P("sp", "tp"),
        P("sp", "tp"),
        P("sp", "tp"),
        P("sp", "tp"),
        P("sp", "tp"),
    )
    return jax.shard_map(body, mesh=mesh, in_specs=in_specs, out_specs=out_specs, check_vma=False)
```

profile of v0, /device:TPU:0, one launch (start us, length us, event | category | flops | bytes accessed | tf_op | source)
XLA Modules:
  0.0 272.4 jit_solution(12463252049788378154)
XLA Ops:
  7.2 0.9 copy.74
  9.7 0.8 dynamic-slice_convert_fusion
  10.5 1.0 multiply_convert_fusion.6
  11.7 1.0 broadcast_in_dim.86
  13.6 2.0 gather_fusion.2
  15.5 2.0 gather_fusion.1
  17.7 21.7 %all_to_all.15 = bf16[8,64,512]{2,1,0:T(8,128)(2,1)} all-to-all(bf16[8,64,512]{2,1,0:T(8,128)(2,1)S(1)} %bitcast.123), channel_id=1, replica_groups=mesh['sp'=8,'tp'=4] {'sp'}, dimensions={0} | all-to-all | bytes 1048576 | tf_op jit(solution)/shard_map/all_to_all | solution.py:144
  39.5 17.6 %all_to_all.16 = bf16[8,64,512]{2,1,0:T(8,128)(2,1)} all-to-all(bf16[8,64,512]{2,1,0:T(8,128)(2,1)S(1)} %bitcast.122), channel_id=1, replica_groups=mesh['sp'=8,'tp'=4] {'sp'}, dimensions={0} | all-to-all | bytes 1048576 | tf_op jit(solution)/shard_map/all_to_all | solution.py:145
  57.4 3.8 %all-gather.7.cloned.1.call-done = bf16[8,64,2048]{2,1,0:T(8,128)(2,1)} async-done(((bf16[8,64,512]{2,1,0:T(8,128)(2,1)}), bf16[8,64,2048]{2,1,0:T(8,128)(2,1)}) %all-gather.7.cloned.1.call-update) | async-done | bytes 2097168 | tf_op jit(solution)/shard_map/all_gather | solution.py:152
  61.2 6.4 %fusion.7 = f32[512,896]{1,0:T(8,128)} fusion(bf16[512,2048]{1,0:T(8,128)(2,1)} %bitcast.142, bf16[1,896,2048]{2,1,0:T(8,128)(2,1)} %param.26), kind=kOutput, calls=%fused_computation.13 | convolution fusion | flops 1879048192 | bytes 7602176 | tf_op jit(solution)/shard_map/dot_general | solution.py:26
  67.6 3.6 %fusion.3 = f32[512,896]{1,0:T(8,128)} fusion(bf16[512,2048]{1,0:T(8,128)(2,1)S(1)} %bitcast.144, bf16[1,896,2048]{2,1,0:T(8,128)(2,1)S(1)} %copy-done.13), kind=kOutput, calls=%fused_computation.9 | convolution fusion | flops 1879048192 | bytes 7602176 | tf_op jit(solution)/shard_map/dot_general | solution.py:26
  71.3 14.1 %all-gather.5.cloned.1.call-done = bf16[8,64,2048]{2,1,0:T(8,128)(2,1)} async-done(((bf16[8,64,512]{2,1,0:T(8,128)(2,1)}), bf16[8,64,2048]{2,1,0:T(8,128)(2,1)}) %all-gather.5.cloned.1.call-update) | async-done | bytes 2097168 | tf_op jit(solution)/shard_map/all_gather | solution.py:153
  85.3 5.8 %multiply_convert_fusion.2 = (bf16[512,896]{1,0:T(8,128)(2,1)S(1)}, f32[512,896]{1,0:T(8,128)S(1)}) fusion(f32[512,896]{1,0:T(8,128)} %fusion.7, bf16[512,2048]{1,0:T(8,128)(2,1)} %bitcast.145, bf16[1,896,2048]{2,1,0:T(8,128)(2,1)} %param.28), kind=kOutput, calls=%fused_computation.22 | convolution fusion | flops 1881800704 | bytes 10354688 | tf_op jit(solution)/shard_map/dot_general | solution.py:26
  91.2 2.3 fusion.1
  94.6 4.1 %add_convert_fusion = bf16[512,2048]{1,0:T(8,128)(2,1)} fusion(f32[512,2048]{1,0:T(8,128)S(1)} %fusion.1, bf16[1,896,2048]{2,1,0:T(8,128)(2,1)S(1)} %copy-done.15, f32[512,896]{1,0:T(8,128)S(1)} %copy-done.19, f32[512,896]{1,0:T(8,128)S(1)} %get-tuple-element.213, f32[512,896]{1,0:T(8,128)S(1)} %copy-done.21), kind=kOutput, calls=%fused_computation.6 | convolution fusion | flops 1885732864 | bytes 15466496 | tf_op jit(solution)/shard_map/dot_general | solution.py:169
  102.1 21.3 %all-reduce.2 = f32[32]{0:T(128)S(1)} all-reduce(f32[32]{0:T(128)S(1)} %dynamic-update-slice), channel_id=3, replica_groups=mesh['sp'=8,'tp'=4] {'sp'}, use_global_device_ids=true, to_apply=%add.2 | all-reduce | flops 32 | bytes 256
  124.1 6.0 %reduce-scatter.3.cloned.1.call-done = bf16[512,512]{1,0:T(8,128)(2,1)} async-done(((bf16[512,2048]{1,0:T(8,128)(2,1)}), bf16[512,512]{1,0:T(8,128)(2,1)}) %reduce-scatter.3.cloned.1.call-update) | async-done | bytes 524304 | tf_op jit(solution)/shard_map/reduce_scatter | solution.py:172
  130.2 5.5 %all-to-all-start.2 = ((bf16[8,64,512]{2,1,0:T(8,128)(2,1)}), bf16[8,64,512]{2,1,0:T(8,128)(2,1)S(1)}, u32[]{:S(2)}, u32[]{:S(2)}) async-start(bf16[8,64,512]{2,1,0:T(8,128)(2,1)} %bitcast.134), calls=%async_computation.3 | async-start | bytes 1048576 | tf_op jit(solution)/shard_map/all_to_all | solution.py:175
  136.0 6.0 %convert_bitcast_fusion.1 = bf16[1,896,2048]{2,1,0:T(8,128)(2,1)} fusion(bf16[512,896]{1,0:T(8,128)(2,1)} %copy-done.23, bf16[512,2048]{1,0:T(8,128)(2,1)} %bitcast.143), kind=kOutput, calls=%fused_computation.18 | convolution fusion | flops 1880883200 | bytes 6684672 | tf_op jit(solution)/shard_map/dot_general | solution.py:32
  141.9 4.0 %convert_bitcast_fusion = bf16[1,896,2048]{2,1,0:T(8,128)(2,1)} fusion(bf16[512,2048]{1,0:T(8,128)(2,1)S(1)} %bitcast.146, f32[512,896]{1,0:T(8,128)S(1)} %copy-done.22, f32[512,896]{1,0:T(8,128)S(1)} %copy-done.20), kind=kOutput, calls=%fused_computation.17 | convolution fusion | flops 1883635712 | bytes 9437184 | tf_op jit(solution)/shard_map/dot_general | solution.py:32
  145.9 4.1 %all-to-all-done.2 = bf16[8,64,512]{2,1,0:T(8,128)(2,1)S(1)} async-done(((bf16[8,64,512]{2,1,0:T(8,128)(2,1)}), bf16[8,64,512]{2,1,0:T(8,128)(2,1)S(1)}, u32[]{:S(2)}, u32[]{:S(2)}) %all-to-all-start.2) | async-done | bytes 524320 | tf_op jit(solution)/shard_map/all_to_all | solution.py:175
  150.0 1.2 gather_fusion
  152.1 5.9 %psum.7 = f32[128]{0:T(128)S(1)} all-reduce(f32[128]{0:T(128)S(1)} %multiply_reduce_fusion), channel_id=1, replica_groups=mesh['sp'=8,'tp'=4] {'tp'}, use_global_device_ids=true, to_apply=%region_8.10 | all-reduce | flops 128 | bytes 1024 | tf_op jit(solution)/shard_map/psum | solution.py:183
  158.2 6.5 %all_gather.21 = bf16[128,2048]{1,0:T(8,128)(2,1)S(1)} all-gather(bf16[128,512]{1,0:T(8,128)(2,1)S(1)} %add_convert_fusion.1), channel_id=1, replica_groups=mesh['sp'=8,'tp'=4] {'tp'}, dimensions={1}, use_global_device_ids=true | all-gather | bytes 655360 | tf_op jit(solution)/shard_map/all_gather | solution.py:188
  165.6 32.8 %all-gather = f32[32,64,64]{2,1,0:T(8,128)S(1)} all-gather(f32[4,64,64]{2,1,0:T(8,128)S(1)} %fusion.30), channel_id=2, replica_groups=mesh['sp'=8,'tp'=4] {'sp'}, dimensions={0}, use_global_device_ids=true | all-gather | bytes 589824 | tf_op jit(solution)/shard_map/all_gather | solution.py:9
  198.4 1.5 convolution_convert_fusion
  199.9 1.1 while.16
  201.5 0.7 copy.87
  203.0 0.7 copy.86
  204.3 0.7 copy.85
  205.1 59.2 %reduce-scatter.5.cloned.1.call-done = bf16[256,256]{1,0:T(8,128)(2,1)} async-done(((bf16[2048,256]{1,0:T(8,128)(2,1)}), bf16[256,256]{1,0:T(8,128)(2,1)}) %reduce-scatter.5.cloned.1.call-update) | async-done | bytes 131088 | tf_op jit(solution)/shard_map/reduce_scatter | solution.py:215
  264.3 1.6 convert_element_type.93
  (132 shorter events, 12.2 us)
Async XLA Ops:
  7.2 157.6 %copy-start = (bf16[256,2048]{1,0:T(8,128)(2,1)S(1)}, bf16[256,2048]{1,0:T(8,128)(2,1)}, u32[]{:S(2)}) copy-start(bf16[256,2048]{1,0:T(8,128)(2,1)} %param.35) | copy-start | bytes 3145732
  7.2 6.0 %copy-start.12 = (f32[128,2]{0,1:T(2,128)S(1)}, f32[128,2]{0,1:T(2,128)}, u32[]{:S(2)}) copy-start(f32[128,2]{0,1:T(2,128)} %param.25) | copy-start | bytes 3076
  7.2 54.0 %all-gather.7.cloned.1.call-start = ((), (), s32[]{:S(2)}) async-start(), calls=%async_computation.6 | async-start | bytes 2621440 | tf_op jit(solution)/shard_map/all_gather | solution.py:152
  39.4 45.9 %all-gather.5.cloned.1.call-start = ((), (), s32[]{:S(2)}) async-start(), calls=%async_computation.5 | async-start | bytes 2621440 | tf_op jit(solution)/shard_map/all_gather | solution.py:153
  57.1 73.0 %reduce-scatter.3.cloned.1.call-start = ((), (), s32[]{:S(2)}) async-start(), calls=%async_computation.7 | async-start | bytes 2621440 | tf_op jit(solution)/shard_map/reduce_scatter | solution.py:172
  61.2 6.5 %copy-start.13 = (bf16[1,896,2048]{2,1,0:T(8,128)(2,1)S(1)}, bf16[1,896,2048]{2,1,0:T(8,128)(2,1)}, u32[]{:S(2)}) copy-start(bf16[1,896,2048]{2,1,0:T(8,128)(2,1)} %param.27) | copy-start | bytes 11010052
  61.2 6.5 %copy-start.16 = (bf16[8,64,2048]{2,1,0:T(8,128)(2,1)S(1)}, bf16[8,64,2048]{2,1,0:T(8,128)(2,1)}, u32[]{:S(2)}) copy-start(bf16[8,64,2048]{2,1,0:T(8,128)(2,1)} %all-gather.7.cloned.1.call-done) | copy-start | bytes 6291460
  85.3 5.8 %copy-start.14 = (bf16[1,896,2048]{2,1,0:T(8,128)(2,1)S(1)}, bf16[1,896,2048]{2,1,0:T(8,128)(2,1)}, u32[]{:S(2)}) copy-start(bf16[1,896,2048]{2,1,0:T(8,128)(2,1)} %param.27) | copy-start | bytes 11010052
  91.1 2.4 copy-start.23
  91.2 2.4 copy-start.15
  91.2 2.9 %copy-start.19 = (f32[512,896]{1,0:T(8,128)S(1)}, f32[512,896]{1,0:T(8,128)}, u32[]{:S(2)}) copy-start(f32[512,896]{1,0:T(8,128)} %fusion.7) | copy-start | bytes 5505028
  91.2 3.5 %copy-start.21 = (f32[512,896]{1,0:T(8,128)S(1)}, f32[512,896]{1,0:T(8,128)}, u32[]{:S(2)}) copy-start(f32[512,896]{1,0:T(8,128)} %fusion.3) | copy-start | bytes 5505028
  98.8 0.7 copy-start.9
  98.8 1.2 copy-start.6
  98.8 1.3 copy-start.11
  98.8 1.6 copy-start.18
  98.8 24.7 %copy-start.7 = (bf16[128,256]{1,0:T(8,128)(2,1)S(1)}, bf16[128,256]{1,0:T(8,128)(2,1)}, u32[]{:S(2)}) copy-start(bf16[128,256]{1,0:T(8,128)(2,1)} %param.30) | copy-start | bytes 196612
  98.8 24.8 %copy-start.8 = (bf16[128,256]{1,0:T(8,128)(2,1)S(1)}, bf16[128,256]{1,0:T(8,128)(2,1)}, u32[]{:S(2)}) copy-start(bf16[128,256]{1,0:T(8,128)(2,1)} %param.31) | copy-start | bytes 196612
  130.2 19.8 %all-to-all-start.2 = ((bf16[8,64,512]{2,1,0:T(8,128)(2,1)}), bf16[8,64,512]{2,1,0:T(8,128)(2,1)S(1)}, u32[]{:S(2)}, u32[]{:S(2)}) async-start(bf16[8,64,512]{2,1,0:T(8,128)(2,1)} %bitcast.134), calls=%async_computation.3 | async-start | bytes 1048576 | tf_op jit(solution)/shard_map/all_to_all | solution.py:175
  135.7 128.6 %reduce-scatter.5.cloned.1.call-start = ((), (), s32[]{:S(2)}) async-start(), calls=%async_computation.8 | async-start | bytes 1179648 | tf_op jit(solution)/shard_map/reduce_scatter | solution.py:215
  135.9 6.0 %copy-start.17 = (bf16[8,64,2048]{2,1,0:T(8,128)(2,1)S(1)}, bf16[8,64,2048]{2,1,0:T(8,128)(2,1)}, u32[]{:S(2)}) copy-start(bf16[8,64,2048]{2,1,0:T(8,128)(2,1)} %all-gather.5.cloned.1.call-done) | copy-start | bytes 6291460
  135.9 6.0 %copy-start.20 = (f32[512,896]{1,0:T(8,128)S(1)}, f32[512,896]{1,0:T(8,128)}, u32[]{:S(2)}) copy-start(f32[512,896]{1,0:T(8,128)} %fusion.7) | copy-start | bytes 5505028
  136.0 6.0 %copy-start.22 = (f32[512,896]{1,0:T(8,128)S(1)}, f32[512,896]{1,0:T(8,128)}, u32[]{:S(2)}) copy-start(f32[512,896]{1,0:T(8,128)} %fusion.3) | copy-start | bytes 5505028
  145.9 6.0 %copy-start.1 = (bf16[128,512]{1,0:T(8,128)(2,1)S(1)}, bf16[128,512]{1,0:T(8,128)(2,1)}, u32[]{:S(2)}) copy-start(bf16[128,512]{1,0:T(8,128)(2,1)} %param.20) | copy-start | bytes 393220
  145.9 6.0 %copy-start.10 = (f32[128]{0:T(128)S(1)}, f32[128]{0:T(128)}, u32[]{:S(2)}) copy-start(f32[128]{0:T(128)} %param.22) | copy-start | bytes 1540
  145.9 12.1 %copy-start.2 = (bf16[128,512]{1,0:T(8,128)(2,1)S(1)}, bf16[128,512]{1,0:T(8,128)(2,1)}, u32[]{:S(2)}) copy-start(bf16[128,512]{1,0:T(8,128)(2,1)} %param.21) | copy-start | bytes 393220
  158.0 40.3 %copy-start.5 = (bf16[128,256]{1,0:T(8,128)(2,1)S(1)}, bf16[128,256]{1,0:T(8,128)(2,1)}, u32[]{:S(2)}) copy-start(bf16[128,256]{1,0:T(8,128)(2,1)} %param.32) | copy-start | bytes 196612
  158.2 41.6 %copy-start.3 = (bf16[128,512]{1,0:T(8,128)(2,1)}, bf16[128,512]{1,0:T(8,128)(2,1)S(1)}, u32[]{:S(2)}) copy-start(bf16[128,512]{1,0:T(8,128)(2,1)S(1)} %add_convert_fusion.1) | copy-start | bytes 393220
  199.9 3.9 %copy-start.4 = (f32[1,4,64,64]{3,2,1,0:T(8,128)S(1)}, f32[1,4,64,64]{3,2,1,0:T(8,128)}, u32[]{:S(2)}) copy-start(f32[1,4,64,64]{3,2,1,0:T(8,128)} %param.34) | copy-start | bytes 196612
Sparse Core Ops, SparseCore 0:
  39.6 21.5 all-gather.6
  62.7 22.5 all-gather.4
  98.9 31.1 reduce-scatter.2
  200.0 64.2 reduce-scatter.4
where the time goes:
time: 273 us; the launch traced here: 272 us
  blocking collectives  106 us (39%)
  waiting for transfers between devices  87.3 us (32%)
  matrix products  36.5 us (13%)
  between operations  15 us (5%)
  local copies, waits for them, and re-layouts  14.6 us (5%)
  other arithmetic  6.82 us (2%)
  starting transfers between devices  6.07 us (2%)
    reduce_scatter x1, waiting for transfers between devices, body(): lax.psum_scatter(contract_first(stream_full, retained).astype(jnp.bfloat1...  59.2 us
    all_gather x1, blocking collectives, prefix(): everything = jax.tree.map(lambda part: lax.all_gather(part, axis), array)  32.8 us
    all_to_all x1, blocking collectives, body(): lax.all_to_all(send_normed, 'sp', split_axis=0, concat_axis=0, tiled=True)  21.7 us
    unnamed x1, blocking collectives  21.3 us
    all_to_all x1, blocking collectives, body(): lax.all_to_all(send_grad, 'sp', split_axis=0, concat_axis=0, tiled=True)  17.6 us
    dot_general x4, matrix products, contract_last(): lax.dot_general(first_op, second_op, (((1,), (1,)), ((), ())), preferred_...  16.3 us
    all_gather x1, waiting for transfers between devices, body(): lax.all_gather(got_grad, 'tp', axis=2, tiled=True)  14.1 us
    dot_general x3, matrix products, contract_first(): lax.dot_general(first_op, second_op, (((0,), (0,)), ((), ())), preferred_...  11.4 us
  transfers between devices with their start and end apart: 5, of which 5 were waited for; matrix products, arithmetic and copies ran while one was open for 10% of the time, Pallas kernels for 0%

commit v1 on v0

--- a/solution.py
+++ b/solution.py
@@ -2,6 +2,12 @@
 import jax.numpy as jnp
 from jax import lax
 from jax.sharding import PartitionSpec as P
+
+
+def gathered_along(array, name, along):
+    blocks = lax.all_gather(array, name, axis=0, tiled=False)
+    out = jnp.concatenate(blocks, axis=along)
+    return out
 
 
 def prefix(array, axis, combine, identity):
@@ -150,7 +156,7 @@
     model_width = gate_weight.shape[1]
     full_normed, full_grad = (
         lax.all_gather(got_normed, "tp", axis=2, tiled=True),
-        lax.all_gather(got_grad, "tp", axis=2, tiled=True),
+        gathered_along(got_grad, "tp", 2),
     )
     normed_rows = full_normed.reshape(-1, model_width)
     grad_rows = full_grad.reshape(-1, model_width)

time: 273 us -> 276 us (1.011)
  matrix products: 36.5 us -> 30.6 us
  waiting for transfers between devices: 87.3 us -> 92.7 us
  local copies, waits for them, and re-layouts: 14.6 us -> 17.7 us
    all_gather x1, waiting for transfers between devices: 3.82 us -> 20.3 us  [body(): lax.all_gather(got_normed, 'tp', axis=2, tiled=True)]
    all_gather x1, waiting for transfers between devices: 14.1 us -> 3.82 us  [gathered_along(): blocks = lax.all_gather(array, name, axis=0, tiled=False)]
    dot_general x4, matrix products: 16.3 us -> 10.5 us  [contract_last(): lax.dot_general(first_op, second_op, (((1,), (1,)), ((), ())), preferred_...]
    all_to_all x1, blocking collectives: 17.6 us -> 21.7 us  [body(): lax.all_to_all(send_grad, 'sp', split_axis=0, concat_axis=0, tiled=True)]
    all_to_all x1, blocking collectives: 21.7 us -> 17.6 us  [body(): lax.all_to_all(send_normed, 'sp', split_axis=0, concat_axis=0, tiled=True)]
    reshape x0 -> x1, local copies, waits for them, and re-layouts: none -> 3.21 us  [gathered_along(): out = jnp.concatenate(blocks, axis=along)]
    unnamed x59 -> x62, local copies, waits for them, and re-layouts: 6.02 us -> 5.82 us
  transfers between devices with their start and end apart: 5 -> 5, of which waited for: 5 -> 5; matrix products, arithmetic and copies ran while one was open for 10% -> 8% of each run, Pallas kernels for 0% -> 0%
where the time goes in v1:
time: 276 us; the launch traced here: 275 us
  blocking collectives  106 us (38%)
  waiting for transfers between devices  92.7 us (34%)
  matrix products  30.6 us (11%)
  local copies, waits for them, and re-layouts  17.7 us (6%)
  between operations  15 us (5%)
  other arithmetic  6.82 us (2%)
  starting transfers between devices  5.84 us (2%)
    reduce_scatter x1, waiting for transfers between devices, body(): lax.psum_scatter(contract_first(stream_full, retained).astype(jnp.bfloat1...  58.3 us
    all_gather x1, blocking collectives, prefix(): everything = jax.tree.map(lambda part: lax.all_gather(part, axis), array)  32.9 us
    all_to_all x1, blocking collectives, body(): lax.all_to_all(send_grad, 'sp', split_axis=0, concat_axis=0, tiled=True)  21.7 us
    unnamed x1, blocking collectives  21.3 us
    all_gather x1, waiting for transfers between devices, body(): lax.all_gather(got_normed, 'tp', axis=2, tiled=True)  20.3 us
    all_to_all x1, blocking collectives, body(): lax.all_to_all(send_normed, 'sp', split_axis=0, concat_axis=0, tiled=True)  17.6 us
    dot_general x3, matrix products, contract_first(): lax.dot_general(first_op, second_op, (((0,), (0,)), ((), ())), preferred_...  11.4 us
    dot_general x4, matrix products, contract_last(): lax.dot_general(first_op, second_op, (((1,), (1,)), ((), ())), preferred_...  10.5 us
  transfers between devices with their start and end apart: 5, of which 5 were waited for; matrix products, arithmetic and copies ran while one was open for 8% of the time, Pallas kernels for 0%

profile of v1, /device:TPU:0, one launch (start us, length us, event | category | flops | bytes accessed | tf_op | source)
XLA Modules:
  0.0 275.1 jit_solution(2423712639898942933)
XLA Ops:
  7.2 0.9 copy.89
  9.7 0.8 dynamic-slice_convert_fusion
  10.5 1.0 multiply_convert_fusion.6
  11.7 1.0 broadcast_in_dim.86
  13.6 2.0 gather_fusion.2
  15.5 2.0 gather_fusion.1
  17.7 21.7 %all_to_all.15 = bf16[8,64,512]{2,1,0:T(8,128)(2,1)} all-to-all(bf16[8,64,512]{2,1,0:T(8,128)(2,1)S(1)} %bitcast.129), channel_id=1, replica_groups=mesh['sp'=8,'tp'=4] {'sp'}, dimensions={0} | all-to-all | bytes 1048576 | tf_op jit(solution)/shard_map/all_to_all | solution.py:151
  39.5 17.6 %all_to_all.16 = bf16[8,64,512]{2,1,0:T(8,128)(2,1)} all-to-all(bf16[8,64,512]{2,1,0:T(8,128)(2,1)S(1)} %bitcast.128), channel_id=1, replica_groups=mesh['sp'=8,'tp'=4] {'sp'}, dimensions={0} | all-to-all | bytes 1048576 | tf_op jit(solution)/shard_map/all_to_all | solution.py:150
  57.4 3.8 %all-gather.8.cloned.1.call-done = bf16[32,64,512]{2,1,0:T(8,128)(2,1)} async-done(((bf16[8,64,512]{2,1,0:T(8,128)(2,1)}), bf16[32,64,512]{2,1,0:T(8,128)(2,1)}) %all-gather.8.cloned.1.call-update) | async-done | bytes 2097168 | tf_op jit(solution)/shard_map/all_gather | solution.py:8
  61.2 3.2 %copy.92 = bf16[8,64,4,512]{3,2,1,0:T(4,128)(2,1)S(1)} copy(bf16[8,64,4,512]{3,1,0,2:T(8,128)(2,1)} %bitcast.132) | data formatting | bytes 4194304 | tf_op jit(solution)/shard_map/reshape | solution.py:9
  65.0 20.3 %all-gather.6.cloned.1.call-done = bf16[8,64,2048]{2,1,0:T(8,128)(2,1)} async-done(((bf16[8,64,512]{2,1,0:T(8,128)(2,1)}), bf16[8,64,2048]{2,1,0:T(8,128)(2,1)}) %all-gather.6.cloned.1.call-update) | async-done | bytes 2097168 | tf_op jit(solution)/shard_map/all_gather | solution.py:158
  85.3 5.2 %fusion.7 = f32[512,896]{1,0:T(8,128)S(1)} fusion(bf16[512,2048]{1,0:T(8,128)(2,1)} %bitcast.151, bf16[1,896,2048]{2,1,0:T(8,128)(2,1)} %param.26), kind=kOutput, calls=%fused_computation.13 | convolution fusion | flops 1879048192 | bytes 7602176 | tf_op jit(solution)/shard_map/dot_general | solution.py:32
  90.6 2.4 fusion.3
  93.3 2.4 multiply_convert_fusion.2
  95.7 2.3 fusion.1
  98.1 4.1 %add_convert_fusion = bf16[512,2048]{1,0:T(8,128)(2,1)} fusion(f32[512,2048]{1,0:T(8,128)S(1)} %fusion.1, bf16[1,896,2048]{2,1,0:T(8,128)(2,1)S(1)} %copy-done.17, f32[512,896]{1,0:T(8,128)S(1)} %fusion.7, f32[512,896]{1,0:T(8,128)S(1)} %get-tuple-element.220, f32[512,896]{1,0:T(8,128)S(1)} %fusion.3), kind=kOutput, calls=%fused_computation.6 | convolution fusion | flops 1885732864 | bytes 15466496 | tf_op jit(solution)/shard_map/dot_general | solution.py:175
  105.7 21.3 %all-reduce.2 = f32[32]{0:T(128)S(1)} all-reduce(f32[32]{0:T(128)S(1)} %dynamic-update-slice), channel_id=4, replica_groups=mesh['sp'=8,'tp'=4] {'sp'}, use_global_device_ids=true, to_apply=%add.2 | all-reduce | flops 32 | bytes 256
  127.7 5.9 %reduce-scatter.3.cloned.1.call-done = bf16[512,512]{1,0:T(8,128)(2,1)} async-done(((bf16[512,2048]{1,0:T(8,128)(2,1)}), bf16[512,512]{1,0:T(8,128)(2,1)}) %reduce-scatter.3.cloned.1.call-update) | async-done | bytes 524304 | tf_op jit(solution)/shard_map/reduce_scatter | solution.py:178
  133.6 5.5 %all-to-all-start.2 = ((bf16[8,64,512]{2,1,0:T(8,128)(2,1)}), bf16[8,64,512]{2,1,0:T(8,128)(2,1)S(1)}, u32[]{:S(2)}, u32[]{:S(2)}) async-start(bf16[8,64,512]{2,1,0:T(8,128)(2,1)} %bitcast.143), calls=%async_computation.3 | async-start | bytes 1048576 | tf_op jit(solution)/shard_map/all_to_all | solution.py:181
  139.2 6.0 %convert_bitcast_fusion.1 = bf16[1,896,2048]{2,1,0:T(8,128)(2,1)} fusion(bf16[512,896]{1,0:T(8,128)(2,1)} %copy-done.24, bf16[512,2048]{1,0:T(8,128)(2,1)} %bitcast.152), kind=kOutput, calls=%fused_computation.18 | convolution fusion | flops 1880883200 | bytes 6684672 | tf_op jit(solution)/shard_map/dot_general | solution.py:38
  145.2 4.0 %convert_bitcast_fusion = bf16[1,896,2048]{2,1,0:T(8,128)(2,1)} fusion(bf16[512,2048]{1,0:T(8,128)(2,1)S(1)} %bitcast.131, f32[512,896]{1,0:T(8,128)S(1)} %copy-done.23, f32[512,896]{1,0:T(8,128)S(1)} %copy-done.21), kind=kOutput, calls=%fused_computation.17 | convolution fusion | flops 1883635712 | bytes 9437184 | tf_op jit(solution)/shard_map/dot_general | solution.py:38
  149.2 4.3 %all-to-all-done.2 = bf16[8,64,512]{2,1,0:T(8,128)(2,1)S(1)} async-done(((bf16[8,64,512]{2,1,0:T(8,128)(2,1)}), bf16[8,64,512]{2,1,0:T(8,128)(2,1)S(1)}, u32[]{:S(2)}, u32[]{:S(2)}) %all-to-all-start.2) | async-done | bytes 524320 | tf_op jit(solution)/shard_map/all_to_all | solution.py:181
  153.5 1.2 gather_fusion
  155.5 5.9 %psum.7 = f32[128]{0:T(128)S(1)} all-reduce(f32[128]{0:T(128)S(1)} %multiply_reduce_fusion), channel_id=1, replica_groups=mesh['sp'=8,'tp'=4] {'tp'}, use_global_device_ids=true, to_apply=%region_8.10 | all-reduce | flops 128 | bytes 1024 | tf_op jit(solution)/shard_map/psum | solution.py:189
  161.6 6.6 %all_gather.25 = bf16[128,2048]{1,0:T(8,128)(2,1)S(1)} all-gather(bf16[128,512]{1,0:T(8,128)(2,1)S(1)} %add_convert_fusion.1), channel_id=1, replica_groups=mesh['sp'=8,'tp'=4] {'tp'}, dimensions={1}, use_global_device_ids=true | all-gather | bytes 655360 | tf_op jit(solution)/shard_map/all_gather | solution.py:194
  169.1 32.9 %all-gather.1 = f32[32,64,64]{2,1,0:T(8,128)S(1)} all-gather(f32[4,64,64]{2,1,0:T(8,128)S(1)} %fusion.30), channel_id=3, replica_groups=mesh['sp'=8,'tp'=4] {'sp'}, dimensions={0}, use_global_device_ids=true | all-gather | bytes 589824 | tf_op jit(solution)/shard_map/all_gather | solution.py:15
  201.9 1.4 convolution_convert_fusion
  203.4 1.1 while.16
  205.1 0.7 copy.103
  206.5 0.7 copy.102
  208.6 58.3 %reduce-scatter.5.cloned.1.call-done = bf16[256,256]{1,0:T(8,128)(2,1)} async-done(((bf16[2048,256]{1,0:T(8,128)(2,1)}), bf16[256,256]{1,0:T(8,128)(2,1)}) %reduce-scatter.5.cloned.1.call-update) | async-done | bytes 131088 | tf_op jit(solution)/shard_map/reduce_scatter | solution.py:221
  266.9 1.6 convert_element_type.93
  (136 shorter events, 12.6 us)
Async XLA Ops:
  7.2 161.0 %copy-start = (bf16[256,2048]{1,0:T(8,128)(2,1)S(1)}, bf16[256,2048]{1,0:T(8,128)(2,1)}, u32[]{:S(2)}) copy-start(bf16[256,2048]{1,0:T(8,128)(2,1)} %param.35) | copy-start | bytes 3145732
  7.2 6.0 %copy-start.14 = (f32[128,2]{0,1:T(2,128)S(1)}, f32[128,2]{0,1:T(2,128)}, u32[]{:S(2)}) copy-start(f32[128,2]{0,1:T(2,128)} %param.25) | copy-start | bytes 3076
  7.2 54.0 %all-gather.8.cloned.1.call-start = ((), (), s32[]{:S(2)}) async-start(), calls=%async_computation.8 | async-start | bytes 2621440 | tf_op jit(solution)/shard_map/all_gather | solution.py:8
  39.4 45.9 %all-gather.6.cloned.1.call-start = ((), (), s32[]{:S(2)}) async-start(), calls=%async_computation.5 | async-start | bytes 2621440 | tf_op jit(solution)/shard_map/all_gather | solution.py:158
  57.1 76.5 %reduce-scatter.3.cloned.1.call-start = ((), (), s32[]{:S(2)}) async-start(), calls=%async_computation.6 | async-start | bytes 2621440 | tf_op jit(solution)/shard_map/reduce_scatter | solution.py:178
  65.0 28.0 %copy-start.1 = (bf16[64,8,4,512]{3,1,2,0:T(8,128)(2,1)}, bf16[64,8,4,512]{3,1,2,0:T(8,128)(2,1)S(1)}, u32[]{:S(2)}) copy-start(bf16[64,8,4,512]{3,1,2,0:T(8,128)(2,1)S(1)} %copy.105) | copy-start | bytes 6291460
  85.3 5.2 %copy-start.16 = (bf16[1,896,2048]{2,1,0:T(8,128)(2,1)S(1)}, bf16[1,896,2048]{2,1,0:T(8,128)(2,1)}, u32[]{:S(2)}) copy-start(bf16[1,896,2048]{2,1,0:T(8,128)(2,1)} %param.27) | copy-start | bytes 11010052
  85.3 5.2 %copy-start.18 = (bf16[8,64,2048]{2,1,0:T(8,128)(2,1)S(1)}, bf16[8,64,2048]{2,1,0:T(8,128)(2,1)}, u32[]{:S(2)}) copy-start(bf16[8,64,2048]{2,1,0:T(8,128)(2,1)} %all-gather.6.cloned.1.call-done) | copy-start | bytes 6291460
  90.6 7.5 %copy-start.20 = (f32[512,896]{1,0:T(8,128)}, f32[512,896]{1,0:T(8,128)S(1)}, u32[]{:S(2)}) copy-start(f32[512,896]{1,0:T(8,128)S(1)} %fusion.7) | copy-start | bytes 5505028
  90.6 2.7 copy-start.15
  93.0 5.1 %copy-start.22 = (f32[512,896]{1,0:T(8,128)}, f32[512,896]{1,0:T(8,128)S(1)}, u32[]{:S(2)}) copy-start(f32[512,896]{1,0:T(8,128)S(1)} %fusion.3) | copy-start | bytes 5505028
  95.7 2.4 copy-start.24
  95.7 2.4 copy-start.17
  102.2 0.7 copy-start.11
  102.2 1.3 copy-start.8
  102.2 1.4 copy-start.13
  102.2 1.8 copy-start.19
  102.2 24.8 %copy-start.9 = (bf16[128,256]{1,0:T(8,128)(2,1)S(1)}, bf16[128,256]{1,0:T(8,128)(2,1)}, u32[]{:S(2)}) copy-start(bf16[128,256]{1,0:T(8,128)(2,1)} %param.30) | copy-start | bytes 196612
  102.3 24.9 %copy-start.10 = (bf16[128,256]{1,0:T(8,128)(2,1)S(1)}, bf16[128,256]{1,0:T(8,128)(2,1)}, u32[]{:S(2)}) copy-start(bf16[128,256]{1,0:T(8,128)(2,1)} %param.31) | copy-start | bytes 196612
  133.6 19.9 %all-to-all-start.2 = ((bf16[8,64,512]{2,1,0:T(8,128)(2,1)}), bf16[8,64,512]{2,1,0:T(8,128)(2,1)S(1)}, u32[]{:S(2)}, u32[]{:S(2)}) async-start(bf16[8,64,512]{2,1,0:T(8,128)(2,1)} %bitcast.143), calls=%async_computation.3 | async-start | bytes 1048576 | tf_op jit(solution)/shard_map/all_to_all | solution.py:181
  139.1 127.8 %reduce-scatter.5.cloned.1.call-start = ((), (), s32[]{:S(2)}) async-start(), calls=%async_computation.7 | async-start | bytes 1179648 | tf_op jit(solution)/shard_map/reduce_scatter | solution.py:221
  139.1 6.0 %copy-start.2 = (bf16[64,8,4,512]{3,1,2,0:T(8,128)(2,1)S(1)}, bf16[64,8,4,512]{3,1,2,0:T(8,128)(2,1)}, u32[]{:S(2)}) copy-start(bf16[64,8,4,512]{3,1,2,0:T(8,128)(2,1)} %copy-done.1) | copy-start | bytes 6291460
  139.2 6.0 %copy-start.21 = (f32[512,896]{1,0:T(8,128)S(1)}, f32[512,896]{1,0:T(8,128)}, u32[]{:S(2)}) copy-start(f32[512,896]{1,0:T(8,128)} %copy-done.20) | copy-start | bytes 5505028
  139.2 6.0 %copy-start.23 = (f32[512,896]{1,0:T(8,128)S(1)}, f32[512,896]{1,0:T(8,128)}, u32[]{:S(2)}) copy-start(f32[512,896]{1,0:T(8,128)} %copy-done.22) | copy-start | bytes 5505028
  149.2 6.2 %copy-start.3 = (bf16[128,512]{1,0:T(8,128)(2,1)S(1)}, bf16[128,512]{1,0:T(8,128)(2,1)}, u32[]{:S(2)}) copy-start(bf16[128,512]{1,0:T(8,128)(2,1)} %param.20) | copy-start | bytes 393220
  149.2 6.2 %copy-start.12 = (f32[128]{0:T(128)S(1)}, f32[128]{0:T(128)}, u32[]{:S(2)}) copy-start(f32[128]{0:T(128)} %param.22) | copy-start | bytes 1540
  149.2 12.3 %copy-start.4 = (bf16[128,512]{1,0:T(8,128)(2,1)S(1)}, bf16[128,512]{1,0:T(8,128)(2,1)}, u32[]{:S(2)}) copy-start(bf16[128,512]{1,0:T(8,128)(2,1)} %param.21) | copy-start | bytes 393220
  161.5 40.5 %copy-start.7 = (bf16[128,256]{1,0:T(8,128)(2,1)S(1)}, bf16[128,256]{1,0:T(8,128)(2,1)}, u32[]{:S(2)}) copy-start(bf16[128,256]{1,0:T(8,128)(2,1)} %param.32) | copy-start | bytes 196612
  161.6 41.7 %copy-start.5 = (bf16[128,512]{1,0:T(8,128)(2,1)}, bf16[128,512]{1,0:T(8,128)(2,1)S(1)}, u32[]{:S(2)}) copy-start(bf16[128,512]{1,0:T(8,128)(2,1)S(1)} %add_convert_fusion.1) | copy-start | bytes 393220
  203.4 3.9 %copy-start.6 = (f32[1,4,64,64]{3,2,1,0:T(8,128)S(1)}, f32[1,4,64,64]{3,2,1,0:T(8,128)}, u32[]{:S(2)}) copy-start(f32[1,4,64,64]{3,2,1,0:T(8,128)} %param.34) | copy-start | bytes 196612
Sparse Core Ops, SparseCore 0:
  39.6 21.5 all-gather.7
  62.7 22.5 all-gather.5
  102.4 31.1 reduce-scatter.2
  203.5 63.3 reduce-scatter.4
